TPU v7x, 32 devices: a whole 2x2x4 slice. The times are simulated.
32 devices in a mesh: grp: 2 (over y), sp: 4 (over z), tp: 4 (over x, core).
Axes of the slice: x: 2, y: 2, z: 4, core: 2. Of those that a mesh axis runs over, the one named last changes fastest.
Arguments:
- queries: bfloat16 [4096, 1024], P(('grp', 'sp'), 'tp'), parts along dimension 0, may hold values from -6 to 6
- memory_keys: bfloat16 [4096, 1024], P(('grp', 'sp'), 'tp'), parts along dimension 0, may hold values from -6 to 6
- memory_values: bfloat16 [4096, 1024], P(('grp', 'sp'), 'tp'), parts along dimension 0, may hold values from -6 to 6
- output_preactivation: bfloat16 [4096, 1024], P(('grp', 'sp'), 'tp'), parts along dimension 0, may hold values from -12 to 12
- input_preactivation: float32 [8, 4096], P('tp', ('grp', 'sp')), parts along dimension 1, may hold values from -6 to 140
- forget_preactivation: float32 [8, 4096], P('tp', ('grp', 'sp')), parts along dimension 1, as said below
- extra_forget_terms: float32 [8, 4096], P('tp', ('grp', 'sp')), parts along dimension 1, may hold values from -1 to 0, as said below
- head_norm_gain: float32 [128], replicated, may hold values from 0.1 to 1.9
- output_projection_matrix: bfloat16 [1024, 2048], P('tp'), may hold values from -0.1875 to 0.1875
- residual: bfloat16 [4096, 2048], P(('grp', 'sp', 'tp')), parts along dimension 0, may hold values from -6 to 6
- feedforward_norm_gain: float32 [2048], replicated, may hold values from 0.1 to 1.9
- feedforward_up_matrix: bfloat16 [2048, 8192], P('sp', 'tp'), may hold values from -0.125 to 0.125
- feedforward_down_matrix: bfloat16 [8192, 2048], P('tp', 'sp'), may hold values from -0.0625 to 0.0625
Outputs:
- layer_out: bfloat16 [4096, 2048], P(('grp', 'sp', 'tp')), parts along dimension 0
There are 2 independent parts, one for each index of `grp`. A program takes and returns all parts, laid end to end along the dimension named above; an argument that names none is the same for every part. Nothing has to cross between parts.
Inputs may be any that keep to these rules, and one draw needn't show every extreme that they name: `forget_preactivation`: forget gate pre-activations. `extra_forget_terms`: extra log forget terms, zero at most positions.
All inputs are finite; a program needn't handle non-finite values.
Results may differ from a plain program's by a relative error of at most 0.018.
Values may be sent and summed in bfloat16 or wider, within the bound.
A program may use at most 64 MiB of HBM per device.

v0:
```python
import jax
import jax.numpy as jnp
from jax import lax
from jax.sharding import PartitionSpec as P

BLOCK = 128
neg_big = -1e30
norm_eps = 1e-06
highest = lax.Precision.HIGHEST


def entering(x, axis, combine, identity):
    length, position = (lax.axis_size(axis), lax.axis_index(axis))
    everything = jax.tree.map(lambda part: lax.all_gather(part, axis), x)
    start = jax.tree.map(
        lambda part, zero: jnp.broadcast_to(jnp.asarray(zero, part.dtype), part.shape), x, identity
    )

    def step(k, before):
        reached = k < position
        new = combine(before, jax.tree.map(lambda part: part[k], everything))
        return jax.tree.map(lambda a, b: jnp.where(reached, a, b), new, before)

    return lax.fori_loop(0, length, step, start)


def rms_norm(tensor, gain_vec):
    mean_sq = jnp.mean(tensor * tensor, axis=-1, keepdims=True)
    return tensor * lax.rsqrt(mean_sq + norm_eps) * gain_vec


def combine(earlier, later):
    total_e, max_e, memory_e = earlier
    total_l, max_l, memory_l = later
    carried = total_l + max_e
    new_max = jnp.maximum(carried, max_l)
    old_part = jnp.exp(carried - new_max)
    new_part = jnp.exp(max_l - new_max)
    return (
        total_e + total_l,
        new_max,
        old_part[..., None, None] * memory_e + new_part[..., None, None] * memory_l,
    )


def block_summary(key_blk, val_blk, gate_blk, decay_logarithm):
    block_total = decay_logarithm[..., -1]
    tail_log = block_total[..., None] - decay_logarithm + gate_blk
    tail_max = jnp.max(tail_log, axis=-1)
    weights = jnp.exp(tail_log - tail_max[..., None])
    memory = jnp.einsum("bhsv,bhsk->bhvk", weights[..., None] * val_blk, key_blk, precision=highest)
    return (block_total, tail_max, memory)


def shards(
    queries,
    memory_keys,
    memory_values,
    output_preactivation,
    input_preactivation,
    forget_preactivation,
    extra_forget_terms,
    head_norm_gain,
    output_projection_matrix,
    residual,
    feedforward_norm_gain,
    feedforward_up_matrix,
    feedforward_down_matrix,
):
    tok_count = queries.shape[0]
    head_count = input_preactivation.shape[0]
    head_dim = queries.shape[1] // head_count
    block_len = BLOCK
    block_count = tok_count // block_len

    def to_blocks(tensor):
        return (
            tensor.astype(jnp.float32)
            .reshape(block_count, block_len, head_count, head_dim)
            .transpose(0, 2, 1, 3)
        )

    def gate_block_list(tensor):
        return tensor.reshape(head_count, block_count, block_len).transpose(1, 0, 2)

    query_blk = to_blocks(queries)
    key_blk = to_blocks(memory_keys) * head_dim ** (-0.5)
    val_blk = to_blocks(memory_values)
    gate_blk = gate_block_list(input_preactivation)
    decay_logarithm = jnp.cumsum(
        gate_block_list(jax.nn.log_sigmoid(forget_preactivation) + extra_forget_terms), axis=-1
    )
    summaries = block_summary(key_blk, val_blk, gate_blk, decay_logarithm)
    zero_heads = jnp.zeros((head_count,), jnp.float32)
    zero_memory = jnp.zeros((head_count, head_dim, head_dim), jnp.float32)
    zero_state = (zero_heads, jnp.full((head_count,), neg_big, jnp.float32), zero_memory)
    prefixes = []
    running = zero_state
    for block_idx in range(block_count):
        prefixes.append(running)
        running = combine(running, tuple((member[block_idx] for member in summaries)))
    before = entering(running, "sp", combine, zero_state)
    anchor = (zero_heads, zero_heads, zero_memory)
    incoming = combine(anchor, before)
    starts = [combine(incoming, prefix) for prefix in prefixes]
    start_max = jnp.stack([each_state[1] for each_state in starts])
    start_memory = jnp.stack([each_state[2] for each_state in starts])
    causal = lax.broadcasted_iota(jnp.int32, (block_len, block_len), 0) >= lax.broadcasted_iota(
        jnp.int32, (block_len, block_len), 1
    )
    log_weight = (
        decay_logarithm[..., :, None] - decay_logarithm[..., None, :] + gate_blk[..., None, :]
    )
    log_weight = jnp.where(causal, log_weight, neg_big)
    carry_log = decay_logarithm + start_max[..., None]
    row_max = jnp.maximum(jnp.max(log_weight, axis=-1), carry_log)
    scores = jnp.einsum("bhtd,bhsd->bhts", query_blk, key_blk, precision=highest) * jnp.exp(
        log_weight - row_max[..., None]
    )
    carry_scale = jnp.exp(carry_log - row_max)
    hidden = jnp.einsum("bhts,bhsv->bhtv", scores, val_blk, precision=highest)
    hidden = hidden + carry_scale[..., None] * jnp.einsum(
        "bhvk,bhtk->bhtv", start_memory, query_blk, precision=highest
    )
    hidden = hidden.transpose(0, 2, 1, 3).reshape(tok_count, head_count, head_dim)
    gated = rms_norm(hidden, head_norm_gain) * jax.nn.sigmoid(
        output_preactivation.astype(jnp.float32).reshape(tok_count, head_count, head_dim)
    )
    mixed = gated.reshape(tok_count, head_count * head_dim).astype(jnp.bfloat16)
    branch = lax.psum_scatter(
        jnp.dot(mixed, output_projection_matrix, preferred_element_type=jnp.float32).astype(
            jnp.bfloat16
        ),
        "tp",
        scatter_dimension=0,
        tiled=True,
    ).astype(jnp.float32)
    mid_state = (residual.astype(jnp.float32) + branch).astype(jnp.bfloat16)
    normed = rms_norm(mid_state.astype(jnp.float32), feedforward_norm_gain).astype(jnp.bfloat16)
    normed_all = lax.all_gather(normed, "tp", axis=0, tiled=True)
    upward = jnp.dot(
        normed_all,
        lax.all_gather(feedforward_up_matrix, "sp", axis=0, tiled=True),
        preferred_element_type=jnp.float32,
    )
    active = jnp.square(jax.nn.relu(upward)).astype(jnp.bfloat16)
    mlp_terms = jnp.dot(
        active,
        lax.all_gather(feedforward_down_matrix, "sp", axis=1, tiled=True),
        preferred_element_type=jnp.float32,
    )
    mlp_sum = lax.psum_scatter(
        mlp_terms.astype(jnp.bfloat16), "tp", scatter_dimension=0, tiled=True
    ).astype(jnp.float32)
    return (mid_state.astype(jnp.float32) + mlp_sum).astype(jnp.bfloat16)


def solution(mesh):
    in_specs = (
        P(("grp", "sp"), "tp"),
        P(("grp", "sp"), "tp"),
        P(("grp", "sp"), "tp"),
        P(("grp", "sp"), "tp"),
        P("tp", ("grp", "sp")),
        P("tp", ("grp", "sp")),
        P("tp", ("grp", "sp")),
        P(),
        P("tp", None),
        P(("grp", "sp", "tp"), None),
        P(),
        P("sp", "tp"),
        P("tp", "sp"),
    )
    out_specs = P(("grp", "sp", "tp"), None)
    return jax.shard_map(shards, mesh=mesh, in_specs=in_specs, out_specs=out_specs, check_vma=False)
```

profile of v0, /device:TPU:0, one launch (start us, length us, event | category | flops | bytes accessed | tf_op | source)
XLA Modules:
  0.0 468.9 jit_solution(10719103995341335332)
XLA Ops:
  6.6 0.8 fusion.50
  7.4 1.2 reduce_window_sum.11
  8.7 0.2 slice_reduce_fusion.3
  9.1 0.9 fusion.65
  10.0 0.8 subtract_exponential_fusion.2
  10.8 12.6 %all-gather.1 = f32[4,1,2]{2,1,0:T(1,128)S(1)} all-gather(f32[1,1,2]{2,1,0:T(1,128)S(1)} %get-tuple-element.255), channel_id=1, replica_groups=mesh['grp'=2,'sp'=4,'tp'=4] {'sp'}, dimensions={0}, use_global_device_ids=true | all-gather | bytes 40 | tf_op jit(solution)/shard_map/all_gather | solution.py:14
  23.5 7.6 %all-gather = f32[4,1,2]{2,1,0:T(1,128)S(1)} all-gather(f32[1,1,2]{2,1,0:T(1,128)S(1)} %get-tuple-element.256), channel_id=1, replica_groups=mesh['grp'=2,'sp'=4,'tp'=4] {'sp'}, dimensions={0}, use_global_device_ids=true | all-gather | bytes 40 | tf_op jit(solution)/shard_map/all_gather | solution.py:14
  31.0 1.0 reshape.306
  32.2 1.0 convert_multiply_fusion.2
  33.2 0.3 mul.301
  33.5 0.7 fusion.22
  34.4 15.0 %all_gather.23 = f32[4,2,128,128]{3,2,1,0:T(8,128)S(1)} all-gather(f32[1,2,128,128]{3,2,1,0:T(8,128)S(1)} %fusion.40), channel_id=1, replica_groups=mesh['grp'=2,'sp'=4,'tp'=4] {'sp'}, dimensions={0}, use_global_device_ids=true | all-gather | bytes 655360 | tf_op jit(solution)/shard_map/all_gather | solution.py:14
  49.4 0.6 while.18
  50.1 0.4 fusion.27
  50.7 0.7 fusion.5
  51.7 0.7 fusion.7
  52.4 0.4 multiply_reduce_fusion
  53.0 0.3 copy.58
  53.3 0.6 mul.356
  53.9 2.1 convolution_convert_fusion
  56.1 31.6 %reduce-scatter.3.cloned.1.call-done = bf16[128,2048]{1,0:T(8,128)(2,1)} async-done(((bf16[512,2048]{1,0:T(8,128)(2,1)}), bf16[128,2048]{1,0:T(8,128)(2,1)}) %reduce-scatter.3.cloned.1.call-update) | async-done | bytes 524304 | tf_op jit(solution)/shard_map/reduce_scatter | solution.py:130
  87.6 1.3 fusion.8
  89.0 2.0 fusion.10
  91.1 0.7 all-gather.8.cloned.1.call-update
  91.8 0.5 all-gather.10.cloned.1.call-update
  92.3 0.2 reduce-scatter.5.cloned.1.call-start
  92.6 21.2 %all-gather.6.cloned.1.call-done = bf16[512,2048]{1,0:T(8,128)(2,1)} async-done(((bf16[128,2048]{1,0:T(8,128)(2,1)}), bf16[512,2048]{1,0:T(8,128)(2,1)}) %all-gather.6.cloned.1.call-update) | async-done | bytes 2097168 | tf_op jit(solution)/shard_map/all_gather | solution.py:140
  113.8 151.2 %all-gather.8.cloned.1.call-done = bf16[2048,2048]{1,0:T(8,128)(2,1)} async-done(((bf16[512,2048]{1,0:T(8,128)(2,1)}), bf16[2048,2048]{1,0:T(8,128)(2,1)}) %all-gather.8.cloned.1.call-update) | async-done | bytes 8388624 | tf_op jit(solution)/shard_map/all_gather | solution.py:143
  265.0 149.3 %all-gather.10.cloned.1.call-done = bf16[2048,2048]{1,0:T(8,128)(2,1)} async-done(((bf16[2048,512]{1,0:T(8,128)(2,1)}), bf16[2048,2048]{1,0:T(8,128)(2,1)}) %all-gather.10.cloned.1.call-update) | async-done | bytes 8388624 | tf_op jit(solution)/shard_map/all_gather | solution.py:149
  414.2 16.5 %convolution_convert_fusion.1 = bf16[512,2048]{1,0:T(8,128)(2,1)} fusion(bf16[2048,2048]{1,0:T(8,128)(2,1)} %all-gather.10.cloned.1.call-done, bf16[512,2048]{1,0:T(8,128)(2,1)} %all-gather.6.cloned.1.call-done, bf16[2048,2048]{1,0:T(8,128)(2,1)} %all-gather.8.cloned.1.call-done), kind=kOutput, calls=%fused_computation.16 | convolution fusion | flops 8594128896 | bytes 20971520 | tf_op jit(solution)/shard_map/dot_general | solution.py:147
  430.8 29.5 %reduce-scatter.5.cloned.1.call-done = bf16[128,2048]{1,0:T(8,128)(2,1)} async-done(((bf16[512,2048]{1,0:T(8,128)(2,1)}), bf16[128,2048]{1,0:T(8,128)(2,1)}) %reduce-scatter.5.cloned.1.call-update) | async-done | bytes 524304 | tf_op jit(solution)/shard_map/reduce_scatter | solution.py:152
  460.3 2.1 fusion.11
  (60 shorter events, 2.1 us)
Async XLA Ops:
  6.5 47.3 %copy-start = (bf16[256,2048]{1,0:T(8,128)(2,1)S(1)}, bf16[256,2048]{1,0:T(8,128)(2,1)}, u32[]{:S(2)}) copy-start(bf16[256,2048]{1,0:T(8,128)(2,1)} %param.23) | copy-start | bytes 3145732
  6.5 43.5 %copy-start.4 = (f32[2,512]{1,0:T(2,128)S(1)}, f32[2,512]{1,0:T(2,128)}, u32[]{:S(2)}) copy-start(f32[2,512]{1,0:T(2,128)} %param.19) | copy-start | bytes 12292
  6.5 44.1 %copy-start.7 = (f32[128]{0:T(128)S(1)}, f32[128]{0:T(128)}, u32[]{:S(2)}) copy-start(f32[128]{0:T(128)} %param.22) | copy-start | bytes 1540
  6.5 44.1 %copy-start.3 = (bf16[512,256]{1,0:T(8,128)(2,1)S(1)}, bf16[512,256]{1,0:T(8,128)(2,1)}, u32[]{:S(2)}) copy-start(bf16[512,256]{1,0:T(8,128)(2,1)} %param.15) | copy-start | bytes 786436
  6.5 81.1 %reduce-scatter.3.cloned.1.call-start = ((), (), s32[]{:S(2)}) async-start(), calls=%async_computation.2 | async-start | bytes 2621440 | tf_op jit(solution)/shard_map/reduce_scatter | solution.py:130
  50.7 3.2 copy-start.6
  53.0 34.7 %copy-start.1 = (bf16[128,2048]{1,0:T(8,128)(2,1)S(1)}, bf16[128,2048]{1,0:T(8,128)(2,1)}, u32[]{:S(2)}) copy-start(bf16[128,2048]{1,0:T(8,128)(2,1)} %param.24) | copy-start | bytes 1572868
  53.9 35.1 %copy-start.5 = (f32[2048]{0:T(1024)S(1)}, f32[2048]{0:T(1024)}, u32[]{:S(2)}) copy-start(f32[2048]{0:T(1024)} %param.25) | copy-start | bytes 24580
  56.0 57.7 %all-gather.6.cloned.1.call-start = ((), (), s32[]{:S(2)}) async-start(), calls=%async_computation.3 | async-start | bytes 2621440 | tf_op jit(solution)/shard_map/all_gather | solution.py:140
  91.0 174.0 %all-gather.8.cloned.1.call-start = ((), (), s32[]{:S(2)}) async-start(), calls=%async_computation.4 | async-start | bytes 10485760 | tf_op jit(solution)/shard_map/all_gather | solution.py:143
  91.8 322.5 %all-gather.10.cloned.1.call-start = ((), (), s32[]{:S(2)}) async-start(), calls=%async_computation.5 | async-start | bytes 10485760 | tf_op jit(solution)/shard_map/all_gather | solution.py:149
  92.3 368.0 %copy-start.2 = (bf16[128,2048]{1,0:T(8,128)(2,1)S(1)}, bf16[128,2048]{1,0:T(8,128)(2,1)}, u32[]{:S(2)}) copy-start(bf16[128,2048]{1,0:T(8,128)(2,1)} %reduce-scatter.3.cloned.1.call-done) | copy-start | bytes 1572868
  92.3 367.9 %reduce-scatter.5.cloned.1.call-start = ((), (), s32[]{:S(2)}) async-start(), calls=%async_computation.6 | async-start | bytes 2621440 | tf_op jit(solution)/shard_map/reduce_scatter | solution.py:152
Sparse Core Ops, SparseCore 0:
  56.1 31.4 reduce-scatter.2
  91.1 22.5 all-gather.5
  115.3 149.6 all-gather.7
  266.4 147.7 all-gather.9
  430.9 29.3 reduce-scatter.4
where the time goes:
time: 469 us
  waiting for transfers between devices  384 us (82%)
  blocking collectives  35.2 us (8%)
  matrix products  21.1 us (4%)
  between operations  13.4 us (3%)
  other arithmetic  11.6 us (2%)
    all_gather x1, waiting for transfers between devices, shards(): lax.all_gather(feedforward_up_matrix, 'sp', axis=0, tiled=True)  151 us
    all_gather x1, waiting for transfers between devices, shards(): lax.all_gather(feedforward_down_matrix, 'sp', axis=1, tiled=True)  149 us
    all_gather x3, blocking collectives, entering(): everything = jax.tree.map(lambda part: lax.all_gather(part, axis), x)  35.2 us
    reduce_scatter x1, waiting for transfers between devices, shards(): lax.psum_scatter(jnp.dot(mixed, output_projection_matrix, preferred_eleme...  31.6 us
    reduce_scatter x1, waiting for transfers between devices, shards(): lax.psum_scatter(mlp_terms.astype(jnp.bfloat16), 'tp', scatter_dimension=...  29.5 us
    all_gather x1, waiting for transfers between devices, shards(): normed_all = lax.all_gather(normed, 'tp', axis=0, tiled=True)  21.2 us
    dot_general x1, matrix products, shards(): jnp.dot(active, lax.all_gather(feedforward_down_matrix, 'sp', axis=1, til...  16.5 us
  transfers between devices with their start and end apart: 5, of which 5 were waited for; matrix products, arithmetic and copies ran while one was open for 0% of the time, Pallas kernels for 0%

commit v1 on v0

--- a/solution.py
+++ b/solution.py
@@ -7,6 +7,11 @@
 neg_big = -1e30
 norm_eps = 1e-06
 highest = lax.Precision.HIGHEST
+
+
+def exchange_gather(x, name, dim):
+    repeated = jnp.stack([x] * lax.axis_size(name))
+    return jnp.concatenate(lax.all_to_all(repeated, name, 0, 0), axis=dim)
 
 
 def entering(x, axis, combine, identity):
@@ -146,7 +151,7 @@
     active = jnp.square(jax.nn.relu(upward)).astype(jnp.bfloat16)
     mlp_terms = jnp.dot(
         active,
-        lax.all_gather(feedforward_down_matrix, "sp", axis=1, tiled=True),
+        exchange_gather(feedforward_down_matrix, "sp", 1),
         preferred_element_type=jnp.float32,
     )
     mlp_sum = lax.psum_scatter(

time: 469 us -> 478 us (1.019)
  local copies, waits for them, and re-layouts: 3.07 us -> 10.3 us
  waiting for transfers between devices: 384 us -> 378 us
  starting transfers between devices: 0.37 us -> 5.94 us
    all_to_all x0 -> x1, waiting for transfers between devices: none -> 308 us  [exchange_gather(): return jnp.concatenate(lax.all_to_all(repeated, name, 0, 0), axis=dim)]
    all_gather x1, waiting for transfers between devices: 151 us -> 0.01 us  [shards(): lax.all_gather(feedforward_up_matrix, 'sp', axis=0, tiled=True)]
    all_gather x1 -> x0, waiting for transfers between devices: 149 us -> none  [shards(): lax.all_gather(feedforward_down_matrix, 'sp', axis=1, tiled=True)]
    all_gather x1, waiting for transfers between devices: 21.2 us -> 8.89 us  [shards(): normed_all = lax.all_gather(normed, 'tp', axis=0, tiled=True)]
    all_to_all x0 -> x1, starting transfers between devices: none -> 5.63 us  [exchange_gather(): return jnp.concatenate(lax.all_to_all(repeated, name, 0, 0), axis=dim)]
  transfers between devices with their start and end apart: 5 -> 5, of which waited for: 5 -> 4; matrix products, arithmetic and copies ran while one was open for 0% -> 2% of each run, Pallas kernels for 0% -> 0%
where the time goes in v1:
time: 478 us
  waiting for transfers between devices  378 us (79%)
  blocking collectives  36.6 us (8%)
  matrix products  21.2 us (4%)
  between operations  13.4 us (3%)
  other arithmetic  11.6 us (2%)
  local copies, waits for them, and re-layouts  10.3 us (2%)
  starting transfers between devices  5.94 us (1%)
    all_to_all x1, waiting for transfers between devices, exchange_gather(): return jnp.concatenate(lax.all_to_all(repeated, name, 0, 0), axis=dim)  308 us
    all_gather x3, blocking collectives, entering(): everything = jax.tree.map(lambda part: lax.all_gather(part, axis), x)  36.6 us
    reduce_scatter x1, waiting for transfers between devices, shards(): lax.psum_scatter(jnp.dot(mixed, output_projection_matrix, preferred_eleme...  30.9 us
    reduce_scatter x1, waiting for transfers between devices, shards(): lax.psum_scatter(mlp_terms.astype(jnp.bfloat16), 'tp', scatter_dimension=...  29.7 us
    dot_general x1, matrix products, shards(): jnp.dot(active, exchange_gather(feedforward_down_matrix, 'sp', 1), prefer...  16.6 us
  transfers between devices with their start and end apart: 5, of which 4 were waited for; matrix products, arithmetic and copies ran while one was open for 2% of the time, Pallas kernels for 0%

profile of v1, /device:TPU:0, one launch (start us, length us, event | category | flops | bytes accessed | tf_op | source)
XLA Modules:
  0.0 477.6 jit_solution(9126041023727417653)
XLA Ops:
  6.5 0.8 fusion.50
  7.4 1.2 reduce_window_sum.11
  9.1 0.8 fusion.65
  9.9 0.8 subtract_exponential_fusion.2
  10.8 1.0 convert_multiply_fusion.2
  11.8 0.3 mul.301
  12.1 1.0 reshape.314
  13.3 0.7 fusion.22
  14.1 17.4 %all_gather.20 = f32[4,2,128,128]{3,2,1,0:T(8,128)S(1)} all-gather(f32[1,2,128,128]{3,2,1,0:T(8,128)S(1)} %fusion.40), channel_id=1, replica_groups=mesh['grp'=2,'sp'=4,'tp'=4] {'sp'}, dimensions={0}, use_global_device_ids=true | all-gather | bytes 655360 | tf_op jit(solution)/shard_map/all_gather | solution.py:19
  31.5 11.7 %all-gather.1 = f32[4,1,2]{2,1,0:T(1,128)S(1)} all-gather(f32[1,1,2]{2,1,0:T(1,128)S(1)} %get-tuple-element.255), channel_id=1, replica_groups=mesh['grp'=2,'sp'=4,'tp'=4] {'sp'}, dimensions={0}, use_global_device_ids=true | all-gather | bytes 40 | tf_op jit(solution)/shard_map/all_gather | solution.py:19
  43.2 7.6 %all-gather = f32[4,1,2]{2,1,0:T(1,128)S(1)} all-gather(f32[1,1,2]{2,1,0:T(1,128)S(1)} %get-tuple-element.256), channel_id=1, replica_groups=mesh['grp'=2,'sp'=4,'tp'=4] {'sp'}, dimensions={0}, use_global_device_ids=true | all-gather | bytes 40 | tf_op jit(solution)/shard_map/all_gather | solution.py:19
  50.7 0.6 while.18
  51.4 0.4 fusion.27
  52.0 0.7 fusion.5
  53.0 0.7 fusion.7
  53.7 0.4 multiply_reduce_fusion
  54.3 0.3 copy.60
  54.6 0.6 mul.356
  55.2 2.1 convolution_convert_fusion
  57.4 30.9 %reduce-scatter.3.cloned.1.call-done = bf16[128,2048]{1,0:T(8,128)(2,1)} async-done(((bf16[512,2048]{1,0:T(8,128)(2,1)}), bf16[128,2048]{1,0:T(8,128)(2,1)}) %reduce-scatter.3.cloned.1.call-update) | async-done | bytes 524304 | tf_op jit(solution)/shard_map/reduce_scatter | solution.py:135
  88.3 1.3 fusion.8
  89.6 2.0 fusion.10
  91.7 2.9 copy.62
  94.7 4.3 stack.47
  98.9 5.6 %all-to-all-start = ((bf16[4,2048,512]{1,2,0:T(8,128)(2,1)}), bf16[4,2048,512]{1,2,0:T(8,128)(2,1)}, u32[]{:S(2)}, u32[]{:S(2)}) async-start(bf16[4,2048,512]{1,2,0:T(8,128)(2,1)} %stack.47), calls=%async_computation.1 | async-start | bytes 16777216 | tf_op jit(solution)/shard_map/all_to_all | solution.py:14
  104.6 0.7 all-gather.7.cloned.1.call-update
  105.3 0.2 reduce-scatter.5.cloned.1.call-start
  105.5 8.9 %all-gather.5.cloned.1.call-done = bf16[512,2048]{1,0:T(8,128)(2,1)} async-done(((bf16[128,2048]{1,0:T(8,128)(2,1)}), bf16[512,2048]{1,0:T(8,128)(2,1)}) %all-gather.5.cloned.1.call-update) | async-done | bytes 2097168 | tf_op jit(solution)/shard_map/all_gather | solution.py:145
  114.4 308.2 %all-to-all-done = bf16[4,2048,512]{1,2,0:T(8,128)(2,1)} async-done(((bf16[4,2048,512]{1,2,0:T(8,128)(2,1)}), bf16[4,2048,512]{1,2,0:T(8,128)(2,1)}, u32[]{:S(2)}, u32[]{:S(2)}) %all-to-all-start) | async-done | bytes 8388640 | tf_op jit(solution)/shard_map/all_to_all | solution.py:14
  422.6 16.6 %convolution_convert_fusion.1 = bf16[512,2048]{1,0:T(8,128)(2,1)} fusion(bf16[2048,2048]{0,1:T(8,128)(2,1)} %bitcast.36, bf16[512,2048]{1,0:T(8,128)(2,1)} %all-gather.5.cloned.1.call-done, bf16[2048,2048]{1,0:T(8,128)(2,1)} %all-gather.7.cloned.1.call-done), kind=kOutput, calls=%fused_computation.16 | convolution fusion | flops 8594128896 | bytes 20971520 | tf_op jit(solution)/shard_map/dot_general | solution.py:152
  439.2 29.7 %reduce-scatter.5.cloned.1.call-done = bf16[128,2048]{1,0:T(8,128)(2,1)} async-done(((bf16[512,2048]{1,0:T(8,128)(2,1)}), bf16[128,2048]{1,0:T(8,128)(2,1)}) %reduce-scatter.5.cloned.1.call-update) | async-done | bytes 524304 | tf_op jit(solution)/shard_map/reduce_scatter | solution.py:157
  469.0 2.1 fusion.11
  (63 shorter events, 2.3 us)
Async XLA Ops:
  6.5 48.7 %copy-start = (bf16[256,2048]{1,0:T(8,128)(2,1)S(1)}, bf16[256,2048]{1,0:T(8,128)(2,1)}, u32[]{:S(2)}) copy-start(bf16[256,2048]{1,0:T(8,128)(2,1)} %param.23) | copy-start | bytes 3145732
  6.5 44.9 %copy-start.5 = (f32[2,512]{1,0:T(2,128)S(1)}, f32[2,512]{1,0:T(2,128)}, u32[]{:S(2)}) copy-start(f32[2,512]{1,0:T(2,128)} %param.19) | copy-start | bytes 12292
  6.5 45.4 %copy-start.4 = (bf16[512,256]{1,0:T(8,128)(2,1)S(1)}, bf16[512,256]{1,0:T(8,128)(2,1)}, u32[]{:S(2)}) copy-start(bf16[512,256]{1,0:T(8,128)(2,1)} %param.15) | copy-start | bytes 786436
  6.5 81.8 %reduce-scatter.3.cloned.1.call-start = ((), (), s32[]{:S(2)}) async-start(), calls=%async_computation.3 | async-start | bytes 2621440 | tf_op jit(solution)/shard_map/reduce_scatter | solution.py:135
  51.4 3.2 copy-start.8
  52.0 3.2 copy-start.7
  54.3 34.0 %copy-start.1 = (bf16[128,2048]{1,0:T(8,128)(2,1)S(1)}, bf16[128,2048]{1,0:T(8,128)(2,1)}, u32[]{:S(2)}) copy-start(bf16[128,2048]{1,0:T(8,128)(2,1)} %param.24) | copy-start | bytes 1572868
  55.2 34.4 %copy-start.6 = (f32[2048]{0:T(1024)S(1)}, f32[2048]{0:T(1024)}, u32[]{:S(2)}) copy-start(f32[2048]{0:T(1024)} %param.25) | copy-start | bytes 24580
  57.4 57.1 %all-gather.5.cloned.1.call-start = ((), (), s32[]{:S(2)}) async-start(), calls=%async_computation.4 | async-start | bytes 2621440 | tf_op jit(solution)/shard_map/all_gather | solution.py:145
  98.9 323.7 %all-to-all-start = ((bf16[4,2048,512]{1,2,0:T(8,128)(2,1)}), bf16[4,2048,512]{1,2,0:T(8,128)(2,1)}, u32[]{:S(2)}, u32[]{:S(2)}) async-start(bf16[4,2048,512]{1,2,0:T(8,128)(2,1)} %stack.47), calls=%async_computation.1 | async-start | bytes 16777216 | tf_op jit(solution)/shard_map/all_to_all | solution.py:14
  104.6 318.0 %all-gather.7.cloned.1.call-start = ((), (), s32[]{:S(2)}) async-start(), calls=%async_computation.5 | async-start | bytes 10485760 | tf_op jit(solution)/shard_map/all_gather | solution.py:148
  105.3 363.7 %reduce-scatter.5.cloned.1.call-start = ((), (), s32[]{:S(2)}) async-start(), calls=%async_computation.6 | async-start | bytes 2621440 | tf_op jit(solution)/shard_map/reduce_scatter | solution.py:157
  422.6 46.4 %copy-start.2 = (bf16[128,2048]{1,0:T(8,128)(2,1)S(1)}, bf16[128,2048]{1,0:T(8,128)(2,1)}, u32[]{:S(2)}) copy-start(bf16[128,2048]{1,0:T(8,128)(2,1)} %param.24) | copy-start | bytes 1572868
  422.6 46.4 %copy-start.3 = (bf16[128,2048]{1,0:T(8,128)(2,1)S(1)}, bf16[128,2048]{1,0:T(8,128)(2,1)}, u32[]{:S(2)}) copy-start(bf16[128,2048]{1,0:T(8,128)(2,1)} %reduce-scatter.3.cloned.1.call-done) | copy-start | bytes 1572868
Sparse Core Ops, SparseCore 0:
  57.5 30.8 reduce-scatter.2
  91.8 22.5 all-gather.4
  116.0 285.3 all-gather.6
  439.4 29.5 reduce-scatter.4
